TPU v7x, 32 devices: a whole 2x2x4 slice. The times are simulated.
32 devices in a mesh: grp: 2 (over y), ep: 8 (over z, x), tp: 2 (over core).
Axes of the slice: x: 2, y: 2, z: 4, core: 2. Of those that a mesh axis runs over, the one named last changes fastest.
Arguments:
- tokens: bfloat16 [384, 2048], P(('grp', 'ep')), parts along dimension 0, may hold values from -6 to 6
- norm_gain: float32 [2048], replicated, may hold values from 0.1 to 1.9
- routes: int32 [384, 4], P(('grp', 'ep')), parts along dimension 0, may hold values from 0 to 7, all different within a row; in each aligned block of 24 rows (0 to 23, 24 to 47, ...) at most 24 rows name the same one
- gate_scores: float32 [384, 4], P(('grp', 'ep')), parts along dimension 0, may hold values from 0.05 to 1
- w_gate: bfloat16 [8, 2048, 512], P('ep', None, 'tp'), may hold values from -1 to 1
- w_up: bfloat16 [8, 2048, 512], P('ep', None, 'tp'), may hold values from -1 to 1
- w_down: bfloat16 [8, 512, 2048], P('ep', 'tp'), may hold values from -0.0625 to 0.0625
Outputs:
- mixed: bfloat16 [384, 2048], P(('grp', 'ep')), parts along dimension 0
There are 2 independent parts, one for each index of `grp`. A program takes and returns all parts, laid end to end along the dimension named above; an argument that names none is the same for every part. Nothing has to cross between parts.
Inputs may be any that keep to these rules, and one draw needn't show every extreme that they name: `routes`: each row names 4 different experts; among the 24 rows of one device no expert is named more than 24 times, a bound that some block reaches.
All inputs are finite; a program needn't handle non-finite values.
Results may differ from a plain program's by a relative error of at most 0.0077.
Values may be sent and summed in bfloat16 or wider, within the bound.
No kernel may reach another device: no remote copies, remote signals or barrier semaphores. Data moves between devices by JAX's collectives and lax.ppermute only.
A program may use at most 64 MiB of HBM per device.

v0:
```python
import jax
import jax.numpy as jnp
from jax import lax
from jax.sharding import PartitionSpec as P


def clamped_unit(g, u):
    gate = jnp.minimum(g, 7.0)
    up = jnp.clip(u, -7.0, 7.0)
    return (up + 1.0) * gate * jax.nn.sigmoid(1.702 * gate)


def expert_rows(rows, wg, wu, wd):
    g = jnp.dot(rows, wg, preferred_element_type=jnp.float32)
    u = jnp.dot(rows, wu, preferred_element_type=jnp.float32)
    act = clamped_unit(g, u).astype(jnp.bfloat16)
    part = jnp.dot(act, wd, preferred_element_type=jnp.float32)
    part = lax.optimization_barrier(part.astype(jnp.bfloat16)).astype(jnp.float32)
    total = lax.psum(part.astype(jnp.bfloat16), "tp")
    return total


def finish(mixed):
    result = mixed.astype(jnp.bfloat16)
    return result


def slot_table(routes, scores, experts, capacity):
    count = routes.shape[0]
    chosen = routes[:, :, None] == experts[None, None, :]
    hit = jnp.any(chosen, axis=1).astype(jnp.int32)
    weight = jnp.sum(jnp.where(chosen, scores[:, :, None], 0.0), axis=1)
    rank = jnp.cumsum(hit, axis=0) - hit
    places = jnp.arange(capacity, dtype=jnp.int32)
    match = (hit[:, :, None] == 1) & (rank[:, :, None] == places[None, None, :])
    row_ids = jnp.arange(count, dtype=jnp.int32)[:, None, None]
    filled = jnp.any(match, axis=0)
    slot_tok = jnp.sum(jnp.where(match, row_ids, 0), axis=0) + count * (
        1 - filled.astype(jnp.int32)
    )
    slot_w = jnp.sum(jnp.where(match, weight[:, :, None], 0.0), axis=0)
    return (slot_tok, slot_w)


def body(tokens, norm_gain, routes, gate_scores, w_gate, w_up, w_down):
    count, width = tokens.shape
    top = routes.shape[1]
    nexp = lax.axis_size("ep")
    capacity = max(2, min(count, 2 * count * top // nexp))
    wg, wu, wd = (w_gate[0], w_up[0], w_down[0])
    xf = tokens.astype(jnp.float32)
    normed = (xf * lax.rsqrt(jnp.mean(xf * xf, axis=-1, keepdims=True) + 1e-06) * norm_gain).astype(
        jnp.bfloat16
    )
    experts = jnp.arange(nexp, dtype=jnp.int32)
    slot_tok, slot_w = slot_table(routes, gate_scores, experts, capacity)
    padded = jnp.concatenate([normed, jnp.zeros((1, width), jnp.bfloat16)], axis=0)
    outgoing = padded[slot_tok]
    received = lax.all_to_all(outgoing, "ep", split_axis=0, concat_axis=0, tiled=True)
    sources, places, _ = received.shape
    outputs = expert_rows(received.reshape(sources * places, width), wg, wu, wd)
    returned = lax.all_to_all(
        outputs.reshape(sources, places, outputs.shape[1]),
        "ep",
        split_axis=0,
        concat_axis=0,
        tiled=True,
    )
    flat_tok = slot_tok.reshape(-1)
    token_ids = jnp.arange(count, dtype=jnp.int32)
    combine = jnp.where(flat_tok[None, :] == token_ids[:, None], slot_w.reshape(-1)[None, :], 0.0)
    mixed = jnp.dot(
        combine,
        returned.reshape(-1, returned.shape[2]).astype(jnp.float32),
        precision=lax.Precision.HIGHEST,
    )
    return finish(mixed)


def solution(mesh):
    in_specs = (
        P(("grp", "ep"), None),
        P(),
        P(("grp", "ep"), None),
        P(("grp", "ep"), None),
        P("ep", None, "tp"),
        P("ep", None, "tp"),
        P("ep", "tp", None),
    )
    out_specs = P(("grp", "ep"), None)
    return jax.shard_map(body, mesh=mesh, in_specs=in_specs, out_specs=out_specs, check_vma=False)
```

profile of v0, /device:TPU:0, one launch (start us, length us, event | category | flops | bytes accessed | tf_op | source)
XLA Modules:
  0.0 94.1 jit_solution(17916535765891462060)
XLA Ops:
  6.5 0.0 copy-start
  6.5 0.0 all-reduce.3.cloned.1.call-start
  6.5 0.8 fusion.23
  7.3 0.1 copy.10
  7.5 0.1 fusion.21
  7.6 0.1 select_reduce_fusion.1
  7.7 1.0 %fusion.8 = f32[24]{0:T(128)S(1)} fusion(bf16[24,2048]{1,0:T(8,128)(2,1)} %param.7), kind=kLoop, calls=%fused_computation.14 | loop fusion | flops 147432 | bytes 98400 | tf_op jit(solution)/shard_map/reduce_sum | solution.py:52
  8.8 0.1 reshape.96
  8.9 1.0 %fusion.10 = bf16[24,2048]{1,0:T(8,128)(2,1)S(1)} fusion(bf16[24,2048]{1,0:T(8,128)(2,1)} %param.7, f32[2048]{0:T(1024)} %param.8, f32[24]{0:T(128)S(1)} %add_rsqrt_fusion), kind=kLoop, calls=%fused_computation.16 | loop fusion | flops 196608 | bytes 204896 | tf_op jit(solution)/shard_map/convert_element_type | solution.py:52
  9.9 1.1 %gather_fusion = bf16[192,2048]{1,0:T(8,128)(2,1)S(1)} fusion(bf16[25,2048]{1,0:T(8,128)(2,1)S(1)} %concatenate.3, s32[1024]{0:T(1024)S(1)} %pad_clamp_fusion), kind=kCustom, calls=%fused_computation | custom fusion | bytes 1573632 | tf_op jit(solution)/shard_map/gather | solution.py:58
  11.0 0.0 copy-start.1
  11.0 27.4 %all_to_all.10 = bf16[8,24,2048]{2,1,0:T(8,128)(2,1)S(1)} all-to-all(bf16[8,24,2048]{2,1,0:T(8,128)(2,1)S(1)} %bitcast.23), channel_id=1, replica_groups=mesh['grp'=2,'ep'=8,'tp'=2] {'ep'}, dimensions={0} | all-to-all | bytes 1572864 | tf_op jit(solution)/shard_map/all_to_all | solution.py:59
  38.4 0.0 copy-start.2
  38.4 0.0 copy-done.1
  38.4 0.4 convolution_minimum_fusion
  38.8 0.0 copy-done
  38.8 0.8 copy-done.2
  39.6 1.9 %convolution_convert_fusion = bf16[192,2048]{1,0:T(8,128)(2,1)} fusion(f32[192,256]{1,0:T(8,128)S(1)} %convolution_minimum_fusion, bf16[192,2048]{1,0:T(8,128)(2,1)S(1)} %bitcast.22, bf16[1,256,2048]{2,1,0:T(8,128)(2,1)S(1)} %copy-done, bf16[1,2048,256]{2,1,0:T(8,128)(2,1)S(1)} %copy-done.2), kind=kOutput, calls=%fused_computation.1 | convolution fusion | flops 403488768 | bytes 3866624 | tf_op jit(solution)/shard_map/dot_general | solution.py:17
  41.6 0.0 copy-start.3
  41.6 0.0 copy-start.4
  41.6 0.0 all-reduce.3.cloned.1.call-update
  41.6 18.2 %all-reduce.3.cloned.1.call-done = bf16[8,24,2048]{2,1,0:T(8,128)(2,1)} async-done(((bf16[8,24,2048]{2,1,0:T(8,128)(2,1)}), bf16[8,24,2048]{2,1,0:T(8,128)(2,1)}) %all-reduce.3.cloned.1.call-update) | async-done | bytes 786448 | tf_op jit(solution)/shard_map/psum | solution.py:19
  59.8 5.8 %all-to-all-start.1 = ((bf16[8,24,2048]{2,1,0:T(8,128)(2,1)}), bf16[8,24,2048]{2,1,0:T(8,128)(2,1)S(1)}, u32[]{:S(2)}, u32[]{:S(2)}) async-start(bf16[8,24,2048]{2,1,0:T(8,128)(2,1)} %all-reduce.3.cloned.1.call-done), calls=%async_computation.1 | async-start | bytes 1572864 | tf_op jit(solution)/shard_map/all_to_all | solution.py:62
  65.6 0.0 copy-done.3
  65.6 0.0 copy-done.4
  65.6 0.1 copy.11
  65.7 0.1 select_reduce_fusion
  65.8 0.1 broadcast_in_dim.69
  65.9 0.1 add.52
  66.0 20.2 %all-to-all-done.1 = bf16[8,24,2048]{2,1,0:T(8,128)(2,1)S(1)} async-done(((bf16[8,24,2048]{2,1,0:T(8,128)(2,1)}), bf16[8,24,2048]{2,1,0:T(8,128)(2,1)S(1)}, u32[]{:S(2)}, u32[]{:S(2)}) %all-to-all-start.1) | async-done | bytes 786464 | tf_op jit(solution)/shard_map/all_to_all | solution.py:62
  86.1 1.1 %convolution_convert_fusion.1 = bf16[24,2048]{1,0:T(8,128)(2,1)} fusion(bf16[192,2048]{1,0:T(8,128)(2,1)S(1)} %bitcast.24, f32[192]{0:T(256)S(1)} %broadcast_in_dim.69, s32[192]{0:T(256)S(1)} %add.52), kind=kOutput, calls=%fused_computation.2 | convolution fusion | flops 113304576 | bytes 886272 | tf_op jit(solution)/shard_map/dot_general | solution.py:72
  (8 shorter events, 0.1 us)
Async XLA Ops:
  6.5 32.3 %copy-start = (bf16[1,256,2048]{2,1,0:T(8,128)(2,1)S(1)}, bf16[1,256,2048]{2,1,0:T(8,128)(2,1)}, u32[]{:S(2)}) copy-start(bf16[1,256,2048]{2,1,0:T(8,128)(2,1)} %param.13) | copy-start | bytes 3145732
  6.5 53.2 %all-reduce.3.cloned.1.call-start = ((), (), s32[]{:S(2)}) async-start(), calls=%async_computation.2 | async-start | bytes 1572864 | tf_op jit(solution)/shard_map/psum | solution.py:19
  11.0 27.4 %copy-start.1 = (bf16[1,2048,256]{2,1,0:T(8,128)(2,1)S(1)}, bf16[1,2048,256]{2,1,0:T(8,128)(2,1)}, u32[]{:S(2)}) copy-start(bf16[1,2048,256]{2,1,0:T(8,128)(2,1)} %param.11) | copy-start | bytes 3145732
  38.4 1.2 %copy-start.2 = (bf16[1,2048,256]{2,1,0:T(8,128)(2,1)S(1)}, bf16[1,2048,256]{2,1,0:T(8,128)(2,1)}, u32[]{:S(2)}) copy-start(bf16[1,2048,256]{2,1,0:T(8,128)(2,1)} %param.12) | copy-start | bytes 3145732
  41.6 24.0 %copy-start.3 = (s32[24,4]{0,1:T(4,128)S(1)}, s32[24,4]{0,1:T(4,128)}, u32[]{:S(2)}) copy-start(s32[24,4]{0,1:T(4,128)} %param.9) | copy-start | bytes 1156
  41.6 24.0 %copy-start.4 = (f32[24,4]{0,1:T(4,128)S(1)}, f32[24,4]{0,1:T(4,128)}, u32[]{:S(2)}) copy-start(f32[24,4]{0,1:T(4,128)} %param.10) | copy-start | bytes 1156
  59.8 26.4 %all-to-all-start.1 = ((bf16[8,24,2048]{2,1,0:T(8,128)(2,1)}), bf16[8,24,2048]{2,1,0:T(8,128)(2,1)S(1)}, u32[]{:S(2)}, u32[]{:S(2)}) async-start(bf16[8,24,2048]{2,1,0:T(8,128)(2,1)} %all-reduce.3.cloned.1.call-done), calls=%async_computation.1 | async-start | bytes 1572864 | tf_op jit(solution)/shard_map/all_to_all | solution.py:62
Sparse Core Ops, SparseCore 0:
  41.7 17.9 all-reduce.2
where the time goes:
time: 94.4 us; the launch traced here: 94.1 us
  waiting for transfers between devices  38.3 us (41%)
  blocking collectives  27.4 us (29%)
  between operations  13.5 us (14%)
  starting transfers between devices  5.81 us (6%)
  matrix products  3.4 us (4%)
  other arithmetic  3.26 us (3%)
  local copies, waits for them, and re-layouts  2.39 us (3%)
    all_to_all x1, blocking collectives, body(): lax.all_to_all(outgoing, 'ep', split_axis=0, concat_axis=0, tiled=True)  27.4 us
    all_to_all x1, waiting for transfers between devices, body(): lax.all_to_all(outputs.reshape(sources, places, outputs.shape[1]), 'ep',...  20.2 us
    psum x1, waiting for transfers between devices, expert_rows(): total = lax.psum(part.astype(jnp.bfloat16), 'tp')  18.2 us
    all_to_all x1, starting transfers between devices, body(): lax.all_to_all(outputs.reshape(sources, places, outputs.shape[1]), 'ep',...  5.81 us
    dot_general x1, matrix products, expert_rows(): part = jnp.dot(act, wd, preferred_element_type=jnp.float32)  1.94 us
  transfers between devices with their start and end apart: 2, of which 2 were waited for; matrix products, arithmetic and copies ran while one was open for 0% of the time, Pallas kernels for 0%

commit v1 on v0

--- a/solution.py
+++ b/solution.py
@@ -16,7 +16,7 @@
     act = clamped_unit(g, u).astype(jnp.bfloat16)
     part = jnp.dot(act, wd, preferred_element_type=jnp.float32)
     part = lax.optimization_barrier(part.astype(jnp.bfloat16)).astype(jnp.float32)
-    total = lax.psum(part.astype(jnp.bfloat16), "tp")
+    total = jnp.sum(lax.all_gather(part.astype(jnp.bfloat16), "tp"), axis=0)
     return total
 
 

time: 94.4 us -> 88.1 us (0.933)
  waiting for transfers between devices: 38.3 us -> 29.2 us
  other arithmetic: 3.26 us -> 6.1 us
    psum x1 -> x0, waiting for transfers between devices: 18.2 us -> none  [expert_rows(): total = lax.psum(part.astype(jnp.bfloat16), 'tp')]
    all_gather x0 -> x1, waiting for transfers between devices: none -> 8.99 us  [expert_rows(): total = jnp.sum(lax.all_gather(part.astype(jnp.bfloat16), 'tp'), axis=0)]
    reduce_sum x0 -> x1, other arithmetic: none -> 2.83 us  [expert_rows(): total = jnp.sum(lax.all_gather(part.astype(jnp.bfloat16), 'tp'), axis=0)]
where the time goes in v1:
time: 88.1 us; the launch traced here: 87.7 us
  waiting for transfers between devices  29.2 us (33%)
  blocking collectives  27.4 us (31%)
  between operations  13.5 us (15%)
  other arithmetic  6.1 us (7%)
  starting transfers between devices  5.78 us (7%)
  matrix products  3.39 us (4%)
  local copies, waits for them, and re-layouts  2.38 us (3%)
    all_to_all x1, blocking collectives, body(): lax.all_to_all(outgoing, 'ep', split_axis=0, concat_axis=0, tiled=True)  27.4 us
    all_to_all x1, waiting for transfers between devices, body(): lax.all_to_all(outputs.reshape(sources, places, outputs.shape[1]), 'ep',...  20.2 us
    all_gather x1, waiting for transfers between devices, expert_rows(): total = jnp.sum(lax.all_gather(part.astype(jnp.bfloat16), 'tp'), axis=0)  8.99 us
    all_to_all x1, starting transfers between devices, body(): lax.all_to_all(outputs.reshape(sources, places, outputs.shape[1]), 'ep',...  5.78 us
    reduce_sum x1, other arithmetic, expert_rows(): total = jnp.sum(lax.all_gather(part.astype(jnp.bfloat16), 'tp'), axis=0)  2.83 us
    dot_general x1, matrix products, expert_rows(): part = jnp.dot(act, wd, preferred_element_type=jnp.float32)  1.93 us
  transfers between devices with their start and end apart: 2, of which 2 were waited for; matrix products, arithmetic and copies ran while one was open for 0% of the time, Pallas kernels for 0%

profile of v1, /device:TPU:0, one launch (start us, length us, event | category | flops | bytes accessed | tf_op | source)
XLA Modules:
  0.0 87.7 jit_solution(7622431958103664555)
XLA Ops:
  6.5 0.0 copy-start
  6.5 0.0 all-gather.3.cloned.1.call-start
  6.5 0.8 fusion.23
  7.3 0.1 copy.10
  7.5 0.1 fusion.21
  7.6 0.1 select_reduce_fusion.1
  7.7 1.0 %fusion.8 = f32[24]{0:T(128)S(1)} fusion(bf16[24,2048]{1,0:T(8,128)(2,1)} %param.7), kind=kLoop, calls=%fused_computation.14 | loop fusion | flops 147432 | bytes 98400 | tf_op jit(solution)/shard_map/reduce_sum | solution.py:52
  8.8 0.1 reshape.96
  8.9 1.0 %fusion.10 = bf16[24,2048]{1,0:T(8,128)(2,1)S(1)} fusion(bf16[24,2048]{1,0:T(8,128)(2,1)} %param.7, f32[2048]{0:T(1024)} %param.8, f32[24]{0:T(128)S(1)} %add_rsqrt_fusion), kind=kLoop, calls=%fused_computation.16 | loop fusion | flops 196608 | bytes 204896 | tf_op jit(solution)/shard_map/convert_element_type | solution.py:52
  9.9 1.1 %gather_fusion = bf16[192,2048]{1,0:T(8,128)(2,1)S(1)} fusion(bf16[25,2048]{1,0:T(8,128)(2,1)S(1)} %concatenate.3, s32[1024]{0:T(1024)S(1)} %pad_clamp_fusion), kind=kCustom, calls=%fused_computation | custom fusion | bytes 1573632 | tf_op jit(solution)/shard_map/gather | solution.py:58
  11.0 0.0 copy-start.1
  11.0 27.4 %all_to_all.10 = bf16[8,24,2048]{2,1,0:T(8,128)(2,1)S(1)} all-to-all(bf16[8,24,2048]{2,1,0:T(8,128)(2,1)S(1)} %bitcast.24), channel_id=1, replica_groups=mesh['grp'=2,'ep'=8,'tp'=2] {'ep'}, dimensions={0} | all-to-all | bytes 1572864 | tf_op jit(solution)/shard_map/all_to_all | solution.py:59
  38.4 0.0 copy-start.2
  38.4 0.0 copy-done.1
  38.4 0.4 convolution_minimum_fusion
  38.8 0.0 copy-done
  38.8 0.8 copy-done.2
  39.6 1.9 %convolution_convert_fusion = bf16[192,2048]{1,0:T(8,128)(2,1)} fusion(f32[192,256]{1,0:T(8,128)S(1)} %convolution_minimum_fusion, bf16[192,2048]{1,0:T(8,128)(2,1)S(1)} %bitcast.23, bf16[1,256,2048]{2,1,0:T(8,128)(2,1)S(1)} %copy-done, bf16[1,2048,256]{2,1,0:T(8,128)(2,1)S(1)} %copy-done.2), kind=kOutput, calls=%fused_computation.1 | convolution fusion | flops 403488768 | bytes 3866624 | tf_op jit(solution)/shard_map/dot_general | solution.py:17
  41.6 0.0 all-gather.3.cloned.1.call-update
  41.6 9.0 %all-gather.3.cloned.1.call-done = bf16[384,2048]{1,0:T(8,128)(2,1)} async-done(((bf16[192,2048]{1,0:T(8,128)(2,1)}), bf16[384,2048]{1,0:T(8,128)(2,1)}) %all-gather.3.cloned.1.call-update) | async-done | bytes 1572880 | tf_op jit(solution)/shard_map/all_gather | solution.py:19
  50.6 0.0 copy-start.3
  50.6 0.0 copy-start.4
  50.6 2.8 %reduce_sum.52 = bf16[192,2048]{1,0:T(8,128)(2,1)} reduce(bf16[2,192,2048]{2,1,0:T(8,128)(2,1)} %bitcast.26, bf16[]{:T(256)} %constant.8.clone.1), dimensions={0}, to_apply=%region_7.8 | reduce | flops 393216 | bytes 2359298 | tf_op jit(solution)/shard_map/reduce_sum | solution.py:19
  53.4 5.8 %all-to-all-start.1 = ((bf16[8,24,2048]{2,1,0:T(8,128)(2,1)}), bf16[8,24,2048]{2,1,0:T(8,128)(2,1)S(1)}, u32[]{:S(2)}, u32[]{:S(2)}) async-start(bf16[8,24,2048]{2,1,0:T(8,128)(2,1)} %bitcast.7), calls=%async_computation.1 | async-start | bytes 1572864 | tf_op jit(solution)/shard_map/all_to_all | solution.py:62
  59.2 0.0 copy-done.3
  59.2 0.0 copy-done.4
  59.2 0.1 copy.11
  59.3 0.1 select_reduce_fusion
  59.4 0.1 broadcast_in_dim.69
  59.5 0.1 add.50
  59.6 20.2 %all-to-all-done.1 = bf16[8,24,2048]{2,1,0:T(8,128)(2,1)S(1)} async-done(((bf16[8,24,2048]{2,1,0:T(8,128)(2,1)}), bf16[8,24,2048]{2,1,0:T(8,128)(2,1)S(1)}, u32[]{:S(2)}, u32[]{:S(2)}) %all-to-all-start.1) | async-done | bytes 786464 | tf_op jit(solution)/shard_map/all_to_all | solution.py:62
  79.8 1.1 %convolution_convert_fusion.1 = bf16[24,2048]{1,0:T(8,128)(2,1)} fusion(bf16[192,2048]{1,0:T(8,128)(2,1)S(1)} %bitcast.25, f32[192]{0:T(256)S(1)} %broadcast_in_dim.69, s32[192]{0:T(256)S(1)} %add.50), kind=kOutput, calls=%fused_computation.2 | convolution fusion | flops 113304576 | bytes 886272 | tf_op jit(solution)/shard_map/dot_general | solution.py:72
  (8 shorter events, 0.1 us)
Async XLA Ops:
  6.5 32.3 %copy-start = (bf16[1,256,2048]{2,1,0:T(8,128)(2,1)S(1)}, bf16[1,256,2048]{2,1,0:T(8,128)(2,1)}, u32[]{:S(2)}) copy-start(bf16[1,256,2048]{2,1,0:T(8,128)(2,1)} %param.13) | copy-start | bytes 3145732
  6.5 44.0 %all-gather.3.cloned.1.call-start = ((), (), s32[]{:S(2)}) async-start(), calls=%async_computation.2 | async-start | bytes 2359296 | tf_op jit(solution)/shard_map/all_gather | solution.py:19
  11.0 27.4 %copy-start.1 = (bf16[1,2048,256]{2,1,0:T(8,128)(2,1)S(1)}, bf16[1,2048,256]{2,1,0:T(8,128)(2,1)}, u32[]{:S(2)}) copy-start(bf16[1,2048,256]{2,1,0:T(8,128)(2,1)} %param.11) | copy-start | bytes 3145732
  38.4 1.2 %copy-start.2 = (bf16[1,2048,256]{2,1,0:T(8,128)(2,1)S(1)}, bf16[1,2048,256]{2,1,0:T(8,128)(2,1)}, u32[]{:S(2)}) copy-start(bf16[1,2048,256]{2,1,0:T(8,128)(2,1)} %param.12) | copy-start | bytes 3145732
  50.6 8.6 %copy-start.3 = (s32[24,4]{0,1:T(4,128)S(1)}, s32[24,4]{0,1:T(4,128)}, u32[]{:S(2)}) copy-start(s32[24,4]{0,1:T(4,128)} %param.9) | copy-start | bytes 1156
  50.6 8.6 %copy-start.4 = (f32[24,4]{0,1:T(4,128)S(1)}, f32[24,4]{0,1:T(4,128)}, u32[]{:S(2)}) copy-start(f32[24,4]{0,1:T(4,128)} %param.10) | copy-start | bytes 1156
  53.4 26.4 %all-to-all-start.1 = ((bf16[8,24,2048]{2,1,0:T(8,128)(2,1)}), bf16[8,24,2048]{2,1,0:T(8,128)(2,1)S(1)}, u32[]{:S(2)}, u32[]{:S(2)}) async-start(bf16[8,24,2048]{2,1,0:T(8,128)(2,1)} %bitcast.7), calls=%async_computation.1 | async-start | bytes 1572864 | tf_op jit(solution)/shard_map/all_to_all | solution.py:62
Sparse Core Ops, SparseCore 0:
  41.7 8.8 all-gather.2
